TPU v7x, 32 devices: a whole 2x2x4 slice. The times are simulated.
32 devices in a mesh: fs: 8 (over z, x), tp: 4 (over y, core).
Axes of the slice: x: 2, y: 2, z: 4, core: 2. Of those that a mesh axis runs over, the one named last changes fastest.
Arguments:
- prompts: bfloat16 [4, 1024, 2048], P('tp'), may hold values from -6 to 6
- gain_first: float32 [2048], P('fs'), may hold values from 0.1 to 1.9
- gate_first: float32 [2048, 5632], P('fs', 'tp'), may hold values from -0.125 to 0.125
- up_first: float32 [2048, 5632], P('fs', 'tp'), may hold values from -0.125 to 0.125
- down_first: float32 [5632, 2048], P('fs', 'tp'), may hold values from -0.078125 to 0.078125
- gain_second: float32 [2048], P('fs'), may hold values from 0.1 to 1.9
- gate_second: float32 [2048, 5632], P('fs', 'tp'), may hold values from -0.125 to 0.125
- up_second: float32 [2048, 5632], P('fs', 'tp'), may hold values from -0.125 to 0.125
- down_second: float32 [5632, 2048], P('fs', 'tp'), may hold values from -0.078125 to 0.078125
Outputs:
- served_gate_first: bfloat16 [2048, 5632], P(None, 'fs')
- served_up_first: bfloat16 [2048, 5632], P(None, 'fs')
- served_down_first: bfloat16 [5632, 2048], P('fs')
- served_gate_second: bfloat16 [2048, 5632], P(None, 'fs')
- served_up_second: bfloat16 [2048, 5632], P(None, 'fs')
- served_down_second: bfloat16 [5632, 2048], P('fs')
- prompt_states: bfloat16 [4, 1024, 2048], P('tp', 'fs')
All inputs are finite; a program needn't handle non-finite values.
Results may differ from a plain program's by a relative error of at most 0.012.
Values may be sent and summed in bfloat16 or wider, within the bound.
A program may use at most 128 MiB of HBM per device.

v0:
```python
import jax
import jax.numpy as jnp
from jax import lax
from jax.sharding import PartitionSpec as P


def normalize(row_block):
    widened = row_block.astype(jnp.float32)
    scaled = widened * lax.rsqrt(jnp.mean(widened * widened, axis=-1, keepdims=True) + 1e-06)
    return scaled.astype(jnp.bfloat16)


def activate(normed, gate_cols, up_cols):
    gate_val = jnp.dot(normed, gate_cols, preferred_element_type=jnp.float32)
    up_val = jnp.dot(normed, up_cols, preferred_element_type=jnp.float32)
    return (jax.nn.silu(gate_val) * up_val).astype(jnp.bfloat16)


def reorder(matrix, outer_count, inner_count):
    total_rows, columns = matrix.shape
    block_rows = total_rows // (outer_count * inner_count)
    shaped = matrix.reshape(outer_count, inner_count, block_rows, columns)
    return jnp.transpose(shaped, (1, 0, 2, 3)).reshape(total_rows, columns)


def per_device(
    prompts,
    gain_first,
    gate_first,
    up_first,
    down_first,
    gain_second,
    gate_second,
    up_second,
    down_second,
):
    fold_gate_a = (gain_first[:, None] * gate_first).astype(jnp.bfloat16)
    fold_up_a = (gain_first[:, None] * up_first).astype(jnp.bfloat16)
    fold_gate_b = (gain_second[:, None] * gate_second).astype(jnp.bfloat16)
    fold_up_b = (gain_second[:, None] * up_second).astype(jnp.bfloat16)
    round_down_a = down_first.astype(jnp.bfloat16)
    round_down_b = down_second.astype(jnp.bfloat16)
    sliced = (
        lax.all_to_all(fold_gate_a, "tp", split_axis=0, concat_axis=1, tiled=True),
        lax.all_to_all(fold_up_a, "tp", split_axis=0, concat_axis=1, tiled=True),
        lax.all_to_all(fold_gate_b, "tp", split_axis=0, concat_axis=1, tiled=True),
        lax.all_to_all(fold_up_b, "tp", split_axis=0, concat_axis=1, tiled=True),
    )
    blocked = (
        lax.all_to_all(sliced[0], "fs", split_axis=1, concat_axis=0, tiled=True),
        lax.all_to_all(sliced[1], "fs", split_axis=1, concat_axis=0, tiled=True),
        lax.all_to_all(sliced[2], "fs", split_axis=1, concat_axis=0, tiled=True),
        lax.all_to_all(sliced[3], "fs", split_axis=1, concat_axis=0, tiled=True),
    )
    collected = (
        lax.all_gather(blocked[0], "tp", axis=0, tiled=True),
        lax.all_gather(blocked[1], "tp", axis=0, tiled=True),
        lax.all_gather(blocked[2], "tp", axis=0, tiled=True),
        lax.all_gather(blocked[3], "tp", axis=0, tiled=True),
    )
    outer_count = lax.axis_size("tp")
    inner_count = lax.axis_size("fs")
    gate_a = reorder(collected[0], outer_count, inner_count)
    up_a = reorder(collected[1], outer_count, inner_count)
    gate_b = reorder(collected[2], outer_count, inner_count)
    up_b = reorder(collected[3], outer_count, inner_count)
    down_a, down_b = (
        lax.all_gather(round_down_a, "tp", axis=1, tiled=True),
        lax.all_gather(round_down_b, "tp", axis=1, tiled=True),
    )
    tokens_in = prompts.reshape(-1, prompts.shape[-1])
    share = tokens_in.shape[0] // lax.axis_size("fs")
    act_first = activate(normalize(tokens_in), gate_a, up_a)
    selected = act_first
    summed = lax.psum_scatter(
        jnp.dot(selected, down_a, preferred_element_type=jnp.float32).astype(jnp.bfloat16),
        "fs",
        scatter_dimension=0,
        tiled=True,
    ).astype(jnp.float32)
    own_rows = lax.dynamic_slice_in_dim(tokens_in, lax.axis_index("fs") * share, share, 0)
    middle = (own_rows.astype(jnp.float32) + 0.5 * summed).astype(jnp.bfloat16)
    act_second = activate(lax.all_gather(normalize(middle), "fs", axis=0, tiled=True), gate_b, up_b)
    selected = act_second
    final_sum = lax.psum_scatter(
        jnp.dot(selected, down_b, preferred_element_type=jnp.float32).astype(jnp.bfloat16),
        "fs",
        scatter_dimension=0,
        tiled=True,
    ).astype(jnp.float32)
    finished = (middle.astype(jnp.float32) + 0.5 * final_sum).astype(jnp.bfloat16)
    return (
        gate_a,
        up_a,
        down_a,
        gate_b,
        up_b,
        down_b,
        finished.reshape(prompts.shape[0], share, prompts.shape[-1]),
    )


def solution(mesh):
    in_specs = (
        P("tp", None, None),
        P("fs"),
        P("fs", "tp"),
        P("fs", "tp"),
        P("fs", "tp"),
        P("fs"),
        P("fs", "tp"),
        P("fs", "tp"),
        P("fs", "tp"),
    )
    out_specs = (
        P(None, "fs"),
        P(None, "fs"),
        P("fs", None),
        P(None, "fs"),
        P(None, "fs"),
        P("fs", None),
        P("tp", "fs", None),
    )
    return jax.shard_map(
        per_device, mesh=mesh, in_specs=in_specs, out_specs=out_specs, check_vma=False
    )
```

profile of v0, /device:TPU:0, one launch (start us, length us, event | category | flops | bytes accessed | tf_op | source)
XLA Modules:
  0.0 561.2 jit_solution(2317630141392950479)
XLA Ops:
  7.2 0.0 all-gather.8.cloned.1.call-start
  7.2 2.1 multiply_convert_fusion.4
  9.3 15.0 %all_to_all.140 = bf16[4,64,1408]{2,1,0:T(8,128)(2,1)S(1)} all-to-all(bf16[4,64,1408]{2,1,0:T(8,128)(2,1)S(1)} %bitcast.74), channel_id=1, replica_groups=mesh['fs'=8,'tp'=4] {'tp'}, dimensions={0} | all-to-all | bytes 1441792 | tf_op jit(solution)/shard_map/all_to_all | solution.py:44
  24.3 0.6 copy.32
  24.8 0.5 all_to_all.107
  25.3 0.1 copy.33
  25.5 25.8 %all_to_all.141 = bf16[64,8,704]{2,0,1:T(8,128)(2,1)} all-to-all(bf16[64,8,704]{2,0,1:T(8,128)(2,1)S(1)} %copy.33), channel_id=1, replica_groups=mesh['fs'=8,'tp'=4] {'fs'}, dimensions={1} | all-to-all | bytes 1441792 | tf_op jit(solution)/shard_map/all_to_all | solution.py:50
  51.2 0.0 all-gather.8.cloned.1.call-update
  51.3 0.0 all-gather.10.cloned.1.call-start
  51.3 18.9 %all_to_all.142 = bf16[4,64,1408]{2,1,0:T(8,128)(2,1)S(1)} all-to-all(bf16[4,64,1408]{2,1,0:T(8,128)(2,1)S(1)} %bitcast.72), channel_id=1, replica_groups=mesh['fs'=8,'tp'=4] {'tp'}, dimensions={0} | all-to-all | bytes 1441792 | tf_op jit(solution)/shard_map/all_to_all | solution.py:45
  70.2 0.6 copy.35
  70.8 0.5 all_to_all.114
  71.2 0.1 copy.36
  71.4 23.3 %all_to_all.143 = bf16[64,8,704]{2,0,1:T(8,128)(2,1)} all-to-all(bf16[64,8,704]{2,0,1:T(8,128)(2,1)S(1)} %copy.36), channel_id=1, replica_groups=mesh['fs'=8,'tp'=4] {'fs'}, dimensions={1} | all-to-all | bytes 1441792 | tf_op jit(solution)/shard_map/all_to_all | solution.py:51
  94.7 0.0 all-gather.10.cloned.1.call-update
  94.7 0.0 all-gather.12.cloned.1.call-start
  94.8 0.9 convert_element_type.70
  95.8 0.0 reduce-scatter.3.cloned.1.call-start
  95.8 3.1 fusion
  98.9 0.0 all-gather.8.cloned.1.call-done
  98.9 2.5 copy.34
  101.4 20.1 %all-gather.10.cloned.1.call-done = bf16[2048,704]{1,0:T(8,128)(2,1)} async-done(((bf16[512,704]{1,0:T(8,128)(2,1)}), bf16[2048,704]{1,0:T(8,128)(2,1)}) %all-gather.10.cloned.1.call-update) | async-done | bytes 2883600 | tf_op jit(solution)/shard_map/all_gather | solution.py:57
  121.5 4.1 copy.37
  125.6 5.0 fusion.4
  130.6 20.1 %all-gather.12.cloned.1.call-done = bf16[704,2048]{1,0:T(8,128)(2,1)} async-done(((bf16[704,512]{1,0:T(8,128)(2,1)}), bf16[704,2048]{1,0:T(8,128)(2,1)}) %all-gather.12.cloned.1.call-update) | async-done | bytes 2883600 | tf_op jit(solution)/shard_map/all_gather | solution.py:68
  150.7 12.6 %convolution_convert_fusion.1 = bf16[1024,2048]{1,0:T(8,128)(2,1)} fusion(bf16[704,2048]{1,0:T(8,128)(2,1)} %all-gather.12.cloned.1.call-done, f32[1024,704]{0,1:T(8,128)} %fusion.4, bf16[2048,704]{1,0:T(8,128)(2,1)} %bitcast.58, bf16[1,1024,2048]{2,1,0:T(8,128)(2,1)} %param.9, f32[1024]{0:T(1024)S(1)} %add_rsqrt_fusion), kind=kOutput, calls=%fused_computation.6 | convolution fusion | flops 5918294016 | bytes 17043456 | tf_op jit(solution)/shard_map/dot_general | solution.py:76
  163.3 0.2 all-gather.14.cloned.1.call-start
  163.5 0.4 copy-done.6
  164.0 2.9 multiply_convert_fusion.2
  166.9 13.3 %all_to_all.144 = bf16[4,64,1408]{2,1,0:T(8,128)(2,1)S(1)} all-to-all(bf16[4,64,1408]{2,1,0:T(8,128)(2,1)S(1)} %bitcast.75), channel_id=1, replica_groups=mesh['fs'=8,'tp'=4] {'tp'}, dimensions={0} | all-to-all | bytes 1441792 | tf_op jit(solution)/shard_map/all_to_all | solution.py:46
  180.2 1.4 copy.38
  181.6 2.4 all_to_all.121
  184.0 1.3 copy.39
  185.3 38.9 %all_to_all.145 = bf16[64,8,704]{2,0,1:T(8,128)(2,1)} all-to-all(bf16[64,8,704]{2,0,1:T(8,128)(2,1)S(1)} %copy.39), channel_id=1, replica_groups=mesh['fs'=8,'tp'=4] {'fs'}, dimensions={1} | all-to-all | bytes 1441792 | tf_op jit(solution)/shard_map/all_to_all | solution.py:52
  224.2 0.0 all-gather.16.cloned.1.call-start
  224.3 14.4 %all_to_all.146 = bf16[4,64,1408]{2,1,0:T(8,128)(2,1)S(1)} all-to-all(bf16[4,64,1408]{2,1,0:T(8,128)(2,1)} %bitcast.73), channel_id=1, replica_groups=mesh['fs'=8,'tp'=4] {'tp'}, dimensions={0} | all-to-all | bytes 1441792 | tf_op jit(solution)/shard_map/all_to_all | solution.py:47
  238.7 1.4 copy.41
  240.1 2.4 all_to_all.128
  242.5 1.3 copy.42
  243.8 39.6 %all_to_all.147 = bf16[64,8,704]{2,0,1:T(8,128)(2,1)} all-to-all(bf16[64,8,704]{2,0,1:T(8,128)(2,1)S(1)} %copy.42), channel_id=1, replica_groups=mesh['fs'=8,'tp'=4] {'fs'}, dimensions={1} | all-to-all | bytes 1441792 | tf_op jit(solution)/shard_map/all_to_all | solution.py:53
  283.4 0.0 all-gather.20.cloned.1.call-start
  283.5 0.4 reduce-scatter.3.cloned.1.call-done
  283.9 1.5 fusion.8
  285.4 0.8 copy-done.2
  286.2 0.9 fusion.9
  287.2 0.0 all-gather.18.cloned.1.call-start
  287.2 2.3 convert_element_type.73
  289.5 0.0 reduce-scatter.5.cloned.1.call-start
  289.6 23.7 %all-gather.14.cloned.1.call-done = bf16[2048,704]{1,0:T(8,128)(2,1)} async-done(((bf16[512,704]{1,0:T(8,128)(2,1)}), bf16[2048,704]{1,0:T(8,128)(2,1)}) %all-gather.14.cloned.1.call-update) | async-done | bytes 2883600 | tf_op jit(solution)/shard_map/all_gather | solution.py:58
  313.3 3.9 copy.40
  317.2 26.1 %all-gather.16.cloned.1.call-done = bf16[2048,704]{1,0:T(8,128)(2,1)} async-done(((bf16[512,704]{1,0:T(8,128)(2,1)}), bf16[2048,704]{1,0:T(8,128)(2,1)}) %all-gather.16.cloned.1.call-update) | async-done | bytes 2883600 | tf_op jit(solution)/shard_map/all_gather | solution.py:59
  343.3 3.9 copy.43
  347.2 71.6 %all-gather.20.cloned.1.call-done = bf16[1024,2048]{1,0:T(8,128)(2,1)} async-done(((bf16[128,2048]{1,0:T(8,128)(2,1)}), bf16[1024,2048]{1,0:T(8,128)(2,1)}) %all-gather.20.cloned.1.call-update) | async-done | bytes 4194320 | tf_op jit(solution)/shard_map/all_gather | solution.py:83
  418.8 7.9 %fusion.16 = f32[1024,704]{0,1:T(8,128)} fusion(bf16[1024,2048]{1,0:T(8,128)(2,1)} %all-gather.20.cloned.1.call-done, bf16[2048,704]{1,0:T(8,128)(2,1)} %bitcast.60), kind=kOutput, calls=%fused_computation.27 | convolution fusion | flops 2952790016 | bytes 9961472 | tf_op jit(solution)/shard_map/dot_general | solution.py:14
  426.7 19.8 %all-gather.18.cloned.1.call-done = bf16[704,2048]{1,0:T(8,128)(2,1)} async-done(((bf16[704,512]{1,0:T(8,128)(2,1)}), bf16[704,2048]{1,0:T(8,128)(2,1)}) %all-gather.18.cloned.1.call-update) | async-done | bytes 2883600 | tf_op jit(solution)/shard_map/all_gather | solution.py:69
  446.5 12.2 %convolution_convert_fusion = bf16[1024,2048]{1,0:T(8,128)(2,1)} fusion(bf16[704,2048]{1,0:T(8,128)(2,1)} %all-gather.18.cloned.1.call-done, f32[1024,704]{0,1:T(8,128)} %fusion.16, bf16[1024,2048]{1,0:T(8,128)(2,1)} %all-gather.20.cloned.1.call-done, bf16[2048,704]{1,0:T(8,128)(2,1)} %bitcast.62), kind=kOutput, calls=%fused_computation.5 | convolution fusion | flops 5912002560 | bytes 17039360 | tf_op jit(solution)/shard_map/dot_general | solution.py:86
  458.7 2.7 copy.44
  461.4 4.7 copy.45
  466.2 2.7 copy.46
  468.8 4.6 copy.47
  473.5 73.7 %reduce-scatter.5.cloned.1.call-done = bf16[128,2048]{1,0:T(8,128)(2,1)} async-done(((bf16[1024,2048]{1,0:T(8,128)(2,1)}), bf16[128,2048]{1,0:T(8,128)(2,1)}) %reduce-scatter.5.cloned.1.call-update) | async-done | bytes 524304 | tf_op jit(solution)/shard_map/reduce_scatter | solution.py:85
  547.2 2.0 fusion.12
  549.2 3.9 copy.50
  553.1 1.6 copy.51
  (21 shorter events, 0.2 us)
Async XLA Ops:
  7.2 91.8 %all-gather.8.cloned.1.call-start = ((), (), s32[]{:S(2)}) async-start(), calls=%async_computation.10 | async-start | bytes 3932160 | tf_op jit(solution)/shard_map/all_gather | solution.py:56
  51.3 70.3 %all-gather.10.cloned.1.call-start = ((), (), s32[]{:S(2)}) async-start(), calls=%async_computation.11 | async-start | bytes 3932160 | tf_op jit(solution)/shard_map/all_gather | solution.py:57
  70.7 24.0 %copy-start.5 = (f32[704,512]{1,0:T(8,128)S(1)}, f32[704,512]{1,0:T(8,128)}, u32[]{:S(2)}) copy-start(f32[704,512]{1,0:T(8,128)} %param.13) | copy-start | bytes 4325380
  94.7 56.0 %all-gather.12.cloned.1.call-start = ((), (), s32[]{:S(2)}) async-start(), calls=%async_computation.12 | async-start | bytes 3604480 | tf_op jit(solution)/shard_map/all_gather | solution.py:68
  95.8 188.1 %reduce-scatter.3.cloned.1.call-start = ((), (), s32[]{:S(2)}) async-start(), calls=%async_computation.16 | async-start | bytes 4718592 | tf_op jit(solution)/shard_map/reduce_scatter | solution.py:75
  121.5 4.1 copy-start.1
  163.3 0.7 copy-start.6
  163.3 150.0 %all-gather.14.cloned.1.call-start = ((), (), s32[]{:S(2)}) async-start(), calls=%async_computation.13 | async-start | bytes 3932160 | tf_op jit(solution)/shard_map/all_gather | solution.py:58
  224.2 119.1 %all-gather.16.cloned.1.call-start = ((), (), s32[]{:S(2)}) async-start(), calls=%async_computation.14 | async-start | bytes 3932160 | tf_op jit(solution)/shard_map/all_gather | solution.py:59
  283.4 135.4 %all-gather.20.cloned.1.call-start = ((), (), s32[]{:S(2)}) async-start(), calls=%async_computation.17 | async-start | bytes 4718592 | tf_op jit(solution)/shard_map/all_gather | solution.py:83
  285.4 0.8 copy-start.2
  287.2 159.4 %all-gather.18.cloned.1.call-start = ((), (), s32[]{:S(2)}) async-start(), calls=%async_computation.15 | async-start | bytes 3604480 | tf_op jit(solution)/shard_map/all_gather | solution.py:69
  289.5 257.7 %reduce-scatter.5.cloned.1.call-start = ((), (), s32[]{:S(2)}) async-start(), calls=%async_computation.18 | async-start | bytes 4718592 | tf_op jit(solution)/shard_map/reduce_scatter | solution.py:85
  461.4 4.7 copy-start
  468.8 78.4 %copy-start.3 = (bf16[128,2048]{1,0:T(8,128)(2,1)S(1)}, bf16[128,2048]{1,0:T(8,128)(2,1)}, u32[]{:S(2)}) copy-start(bf16[128,2048]{1,0:T(8,128)(2,1)} %copy-done.2) | copy-start | bytes 1572868
  549.2 3.9 copy-start.4
Sparse Core Ops, SparseCore 0:
  51.4 31.6 all-gather.7
  94.9 26.6 all-gather.9
  123.7 27.0 all-gather.11
  163.4 120.3 reduce-scatter.2
  285.3 28.0 all-gather.13
  314.7 28.4 all-gather.15
  346.0 72.7 all-gather.19
  420.9 25.5 all-gather.17
  458.9 88.2 reduce-scatter.4
where the time goes:
time: 562 us; the launch traced here: 561 us
  waiting for transfers between devices  256 us (46%)
  blocking collectives  189 us (34%)
  local copies, waits for them, and re-layouts  48.3 us (9%)
  matrix products  37.7 us (7%)
  other arithmetic  15.8 us (3%)
  between operations  14 us (2%)
    reduce_scatter x1, waiting for transfers between devices, per_device(): lax.psum_scatter(jnp.dot(selected, down_b, preferred_element_type=jnp.flo...  73.7 us
    all_gather x1, waiting for transfers between devices, per_device(): lax.all_gather(normalize(middle), 'fs', axis=0, tiled=True)  71.6 us
    all_to_all x1, blocking collectives, per_device(): lax.all_to_all(sliced[3], 'fs', split_axis=1, concat_axis=0, tiled=True)  39.6 us
    all_to_all x1, blocking collectives, per_device(): lax.all_to_all(sliced[2], 'fs', split_axis=1, concat_axis=0, tiled=True)  38.9 us
    all_gather x1, waiting for transfers between devices, per_device(): lax.all_gather(blocked[3], 'tp', axis=0, tiled=True)  26.1 us
    all_to_all x1, blocking collectives, per_device(): lax.all_to_all(sliced[0], 'fs', split_axis=1, concat_axis=0, tiled=True)  25.8 us
    all_gather x1, waiting for transfers between devices, per_device(): lax.all_gather(blocked[2], 'tp', axis=0, tiled=True)  23.7 us
    all_to_all x1, blocking collectives, per_device(): lax.all_to_all(sliced[1], 'fs', split_axis=1, concat_axis=0, tiled=True)  23.3 us
  transfers between devices with their start and end apart: 9, of which 8 were waited for; matrix products, arithmetic and copies ran while one was open for 11% of the time, Pallas kernels for 0%

commit v1 on v0

--- a/solution.py
+++ b/solution.py
@@ -2,6 +2,11 @@
 import jax.numpy as jnp
 from jax import lax
 from jax.sharding import PartitionSpec as P
+
+
+def gather_over(x, axis, dim):
+    repeated = jnp.stack([x] * lax.axis_size(axis))
+    return jnp.concatenate(lax.all_to_all(repeated, axis, 0, 0), axis=dim)
 
 
 def normalize(row_block):
@@ -80,7 +85,7 @@
     ).astype(jnp.float32)
     own_rows = lax.dynamic_slice_in_dim(tokens_in, lax.axis_index("fs") * share, share, 0)
     middle = (own_rows.astype(jnp.float32) + 0.5 * summed).astype(jnp.bfloat16)
-    act_second = activate(lax.all_gather(normalize(middle), "fs", axis=0, tiled=True), gate_b, up_b)
+    act_second = activate(gather_over(normalize(middle), "fs", 0), gate_b, up_b)
     selected = act_second
     final_sum = lax.psum_scatter(
         jnp.dot(selected, down_b, preferred_element_type=jnp.float32).astype(jnp.bfloat16),

time: 562 us -> 510 us (0.907)
  blocking collectives: 189 us -> 150 us
  waiting for transfers between devices: 256 us -> 231 us
  starting transfers between devices: 0.55 us -> 9.32 us
    all_to_all x0 -> x2, waiting for transfers between devices: none -> 74.6 us  [the longest x1 40.1 us: gather_over(): return jnp.concatenate(lax.all_to_all(repeated, axis, 0, 0), axis=dim)]
    all_gather x1 -> x0, waiting for transfers between devices: 71.6 us -> none  [per_device(): lax.all_gather(normalize(middle), 'fs', axis=0, tiled=True)]
    all_to_all x1 -> x0, blocking collectives: 39.6 us -> none  [per_device(): lax.all_to_all(sliced[3], 'fs', split_axis=1, concat_axis=0, tiled=True)]
    all_gather x1, waiting for transfers between devices: 19.8 us -> 0.01 us  [per_device(): lax.all_gather(round_down_b, 'tp', axis=1, tiled=True)]
    all_to_all x0 -> x2, starting transfers between devices: none -> 8.81 us  [the longest x1 4.6 us: gather_over(): return jnp.concatenate(lax.all_to_all(repeated, axis, 0, 0), axis=dim)]
    all_gather x1, waiting for transfers between devices: 23.7 us -> 17.2 us  [per_device(): lax.all_gather(blocked[2], 'tp', axis=0, tiled=True)]
  transfers between devices with their start and end apart: 9 -> 10, of which waited for: 8 -> 7; matrix products, arithmetic and copies ran while one was open for 11% -> 12% of each run, Pallas kernels for 0% -> 0%
where the time goes in v1:
time: 510 us; the launch traced here: 509 us
  waiting for transfers between devices  231 us (45%)
  blocking collectives  150 us (29%)
  local copies, waits for them, and re-layouts  51.7 us (10%)
  matrix products  37.7 us (7%)
  other arithmetic  15 us (3%)
  between operations  14.3 us (3%)
  starting transfers between devices  9.32 us (2%)
    reduce_scatter x1, waiting for transfers between devices, per_device(): lax.psum_scatter(jnp.dot(selected, down_b, preferred_element_type=jnp.flo...  72.7 us
    all_to_all x1, waiting for transfers between devices, gather_over(): return jnp.concatenate(lax.all_to_all(repeated, axis, 0, 0), axis=dim)  40.1 us
    all_to_all x1, blocking collectives, per_device(): lax.all_to_all(sliced[2], 'fs', split_axis=1, concat_axis=0, tiled=True)  38.9 us
    all_to_all x1, waiting for transfers between devices, per_device(): lax.all_to_all(sliced[3], 'fs', split_axis=1, concat_axis=0, tiled=True)  34.5 us
    all_gather x1, waiting for transfers between devices, per_device(): lax.all_gather(blocked[3], 'tp', axis=0, tiled=True)  26.1 us
    all_to_all x1, blocking collectives, per_device(): lax.all_to_all(sliced[0], 'fs', split_axis=1, concat_axis=0, tiled=True)  25.8 us
    all_to_all x1, blocking collectives, per_device(): lax.all_to_all(sliced[1], 'fs', split_axis=1, concat_axis=0, tiled=True)  23.3 us
    unnamed x20, local copies, waits for them, and re-layouts  21.5 us
  transfers between devices with their start and end apart: 10, of which 7 were waited for; matrix products, arithmetic and copies ran while one was open for 12% of the time, Pallas kernels for 0%

profile of v1, /device:TPU:0, one launch (start us, length us, event | category | flops | bytes accessed | tf_op | source)
XLA Modules:
  0.0 508.6 jit_solution(13658312802603450785)
XLA Ops:
  7.2 0.0 all-gather.7.cloned.1.call-start
  7.2 2.1 multiply_convert_fusion.4
  9.3 15.0 %all_to_all.145 = bf16[4,64,1408]{2,1,0:T(8,128)(2,1)S(1)} all-to-all(bf16[4,64,1408]{2,1,0:T(8,128)(2,1)S(1)} %bitcast.74), channel_id=1, replica_groups=mesh['fs'=8,'tp'=4] {'tp'}, dimensions={0} | all-to-all | bytes 1441792 | tf_op jit(solution)/shard_map/all_to_all | solution.py:49
  24.3 0.6 copy.32
  24.8 0.5 all_to_all.110
  25.3 0.1 copy.33
  25.5 25.8 %all_to_all.146 = bf16[64,8,704]{2,0,1:T(8,128)(2,1)} all-to-all(bf16[64,8,704]{2,0,1:T(8,128)(2,1)S(1)} %copy.33), channel_id=1, replica_groups=mesh['fs'=8,'tp'=4] {'fs'}, dimensions={1} | all-to-all | bytes 1441792 | tf_op jit(solution)/shard_map/all_to_all | solution.py:55
  51.3 0.0 all-gather.9.cloned.1.call-start
  51.3 18.9 %all_to_all.147 = bf16[4,64,1408]{2,1,0:T(8,128)(2,1)S(1)} all-to-all(bf16[4,64,1408]{2,1,0:T(8,128)(2,1)S(1)} %bitcast.72), channel_id=1, replica_groups=mesh['fs'=8,'tp'=4] {'tp'}, dimensions={0} | all-to-all | bytes 1441792 | tf_op jit(solution)/shard_map/all_to_all | solution.py:50
  70.2 0.6 copy.35
  70.8 0.5 all_to_all.117
  71.2 0.1 copy.36
  71.4 23.3 %all_to_all.148 = bf16[64,8,704]{2,0,1:T(8,128)(2,1)} all-to-all(bf16[64,8,704]{2,0,1:T(8,128)(2,1)S(1)} %copy.36), channel_id=1, replica_groups=mesh['fs'=8,'tp'=4] {'fs'}, dimensions={1} | all-to-all | bytes 1441792 | tf_op jit(solution)/shard_map/all_to_all | solution.py:56
  94.7 0.0 all-gather.11.cloned.1.call-start
  94.8 0.9 convert_element_type.70
  95.8 0.0 reduce-scatter.3.cloned.1.call-start
  95.8 3.1 fusion
  98.9 0.0 all-gather.7.cloned.1.call-done
  98.9 2.5 copy.34
  101.4 20.1 %all-gather.9.cloned.1.call-done = bf16[2048,704]{1,0:T(8,128)(2,1)} async-done(((bf16[512,704]{1,0:T(8,128)(2,1)}), bf16[2048,704]{1,0:T(8,128)(2,1)}) %all-gather.9.cloned.1.call-update) | async-done | bytes 2883600 | tf_op jit(solution)/shard_map/all_gather | solution.py:62
  121.5 4.1 copy.37
  125.6 5.0 fusion.4
  130.6 20.1 %all-gather.11.cloned.1.call-done = bf16[704,2048]{1,0:T(8,128)(2,1)} async-done(((bf16[704,512]{1,0:T(8,128)(2,1)}), bf16[704,2048]{1,0:T(8,128)(2,1)}) %all-gather.11.cloned.1.call-update) | async-done | bytes 2883600 | tf_op jit(solution)/shard_map/all_gather | solution.py:73
  150.7 12.6 %convolution_convert_fusion.1 = bf16[1024,2048]{1,0:T(8,128)(2,1)} fusion(bf16[704,2048]{1,0:T(8,128)(2,1)} %all-gather.11.cloned.1.call-done, f32[1024,704]{0,1:T(8,128)} %fusion.4, bf16[2048,704]{1,0:T(8,128)(2,1)} %bitcast.59, bf16[1,1024,2048]{2,1,0:T(8,128)(2,1)} %param.9, f32[1024]{0:T(1024)S(1)} %add_rsqrt_fusion), kind=kOutput, calls=%fused_computation.6 | convolution fusion | flops 5918294016 | bytes 17043456 | tf_op jit(solution)/shard_map/dot_general | solution.py:81
  163.3 0.2 all-gather.13.cloned.1.call-start
  163.6 0.4 copy-done.6
  164.0 2.9 multiply_convert_fusion.2
  166.9 13.3 %all_to_all.149 = bf16[4,64,1408]{2,1,0:T(8,128)(2,1)S(1)} all-to-all(bf16[4,64,1408]{2,1,0:T(8,128)(2,1)S(1)} %bitcast.75), channel_id=1, replica_groups=mesh['fs'=8,'tp'=4] {'tp'}, dimensions={0} | all-to-all | bytes 1441792 | tf_op jit(solution)/shard_map/all_to_all | solution.py:51
  180.2 1.4 copy.38
  181.6 2.4 all_to_all.124
  184.0 1.3 copy.39
  185.3 38.9 %all_to_all.150 = bf16[64,8,704]{2,0,1:T(8,128)(2,1)} all-to-all(bf16[64,8,704]{2,0,1:T(8,128)(2,1)S(1)} %copy.39), channel_id=1, replica_groups=mesh['fs'=8,'tp'=4] {'fs'}, dimensions={1} | all-to-all | bytes 1441792 | tf_op jit(solution)/shard_map/all_to_all | solution.py:57
  224.2 0.0 all-gather.13.cloned.1.call-update
  224.2 14.4 %all_to_all.151 = bf16[4,64,1408]{2,1,0:T(8,128)(2,1)S(1)} all-to-all(bf16[4,64,1408]{2,1,0:T(8,128)(2,1)} %bitcast.73), channel_id=1, replica_groups=mesh['fs'=8,'tp'=4] {'tp'}, dimensions={0} | all-to-all | bytes 1441792 | tf_op jit(solution)/shard_map/all_to_all | solution.py:52
  238.6 1.4 copy.41
  240.1 2.4 all_to_all.131
  242.5 2.1 copy.42
  244.6 4.2 all-to-all-start.7
  248.8 0.0 all-gather.15.cloned.1.call-start
  248.9 34.5 %all-to-all-done.7 = bf16[64,8,704]{2,0,1:T(8,128)(2,1)} async-done(((bf16[64,8,704]{2,0,1:T(8,128)(2,1)}), bf16[64,8,704]{2,0,1:T(8,128)(2,1)}, u32[]{:S(2)}, u32[]{:S(2)}) %all-to-all-start.7) | async-done | bytes 720928 | tf_op jit(solution)/shard_map/all_to_all | solution.py:58
  283.5 0.0 reduce-scatter.3.cloned.1.call-done
  283.5 1.5 fusion.8
  285.0 0.8 copy-done.2
  285.8 0.2 fusion.9
  286.0 2.6 stack.2
  288.5 4.6 all-to-all-start.8
  293.1 0.0 all-gather.17.cloned.1.call-start
  293.2 2.3 convert_element_type.73
  295.5 0.0 reduce-scatter.5.cloned.1.call-start
  295.5 17.2 %all-gather.13.cloned.1.call-done = bf16[2048,704]{1,0:T(8,128)(2,1)} async-done(((bf16[512,704]{1,0:T(8,128)(2,1)}), bf16[2048,704]{1,0:T(8,128)(2,1)}) %all-gather.13.cloned.1.call-update) | async-done | bytes 2883600 | tf_op jit(solution)/shard_map/all_gather | solution.py:63
  312.8 3.8 copy.40
  316.6 26.1 %all-gather.15.cloned.1.call-done = bf16[2048,704]{1,0:T(8,128)(2,1)} async-done(((bf16[512,704]{1,0:T(8,128)(2,1)}), bf16[2048,704]{1,0:T(8,128)(2,1)}) %all-gather.15.cloned.1.call-update) | async-done | bytes 2883600 | tf_op jit(solution)/shard_map/all_gather | solution.py:64
  342.7 3.9 copy.43
  346.6 40.1 %all-to-all-done.8 = bf16[8,128,2048]{2,1,0:T(8,128)(2,1)} async-done(((bf16[8,128,2048]{2,1,0:T(8,128)(2,1)}), bf16[8,128,2048]{2,1,0:T(8,128)(2,1)}, u32[]{:S(2)}, u32[]{:S(2)}) %all-to-all-start.8) | async-done | bytes 4194336 | tf_op jit(solution)/shard_map/all_to_all | solution.py:9
  386.7 7.9 %fusion.16 = f32[1024,704]{0,1:T(8,128)} fusion(bf16[1024,2048]{1,0:T(8,128)(2,1)} %bitcast.30, bf16[2048,704]{1,0:T(8,128)(2,1)} %bitcast.61), kind=kOutput, calls=%fused_computation.27 | convolution fusion | flops 2952790016 | bytes 9961472 | tf_op jit(solution)/shard_map/dot_general | solution.py:19
  394.6 12.2 %convolution_convert_fusion = bf16[1024,2048]{1,0:T(8,128)(2,1)} fusion(bf16[704,2048]{1,0:T(8,128)(2,1)} %all-gather.17.cloned.1.call-done, f32[1024,704]{0,1:T(8,128)} %fusion.16, bf16[1024,2048]{1,0:T(8,128)(2,1)} %bitcast.30, bf16[2048,704]{1,0:T(8,128)(2,1)} %bitcast.63), kind=kOutput, calls=%fused_computation.5 | convolution fusion | flops 5912002560 | bytes 17039360 | tf_op jit(solution)/shard_map/dot_general | solution.py:91
  406.8 2.7 copy.44
  409.5 4.7 copy.45
  414.3 2.7 copy.46
  417.0 4.6 copy.47
  421.6 72.7 %reduce-scatter.5.cloned.1.call-done = bf16[128,2048]{1,0:T(8,128)(2,1)} async-done(((bf16[1024,2048]{1,0:T(8,128)(2,1)}), bf16[128,2048]{1,0:T(8,128)(2,1)}) %reduce-scatter.5.cloned.1.call-update) | async-done | bytes 524304 | tf_op jit(solution)/shard_map/reduce_scatter | solution.py:90
  494.3 2.0 fusion.12
  496.2 3.9 copy.50
  500.2 1.6 copy.51
  (22 shorter events, 0.2 us)
Async XLA Ops:
  7.2 91.8 %all-gather.7.cloned.1.call-start = ((), (), s32[]{:S(2)}) async-start(), calls=%async_computation.11 | async-start | bytes 3932160 | tf_op jit(solution)/shard_map/all_gather | solution.py:61
  51.3 70.3 %all-gather.9.cloned.1.call-start = ((), (), s32[]{:S(2)}) async-start(), calls=%async_computation.12 | async-start | bytes 3932160 | tf_op jit(solution)/shard_map/all_gather | solution.py:62
  70.7 24.0 %copy-start.5 = (f32[704,512]{1,0:T(8,128)S(1)}, f32[704,512]{1,0:T(8,128)}, u32[]{:S(2)}) copy-start(f32[704,512]{1,0:T(8,128)} %param.13) | copy-start | bytes 4325380
  94.7 56.0 %all-gather.11.cloned.1.call-start = ((), (), s32[]{:S(2)}) async-start(), calls=%async_computation.13 | async-start | bytes 3604480 | tf_op jit(solution)/shard_map/all_gather | solution.py:73
  95.8 187.7 %reduce-scatter.3.cloned.1.call-start = ((), (), s32[]{:S(2)}) async-start(), calls=%async_computation.17 | async-start | bytes 4718592 | tf_op jit(solution)/shard_map/reduce_scatter | solution.py:80
  121.5 4.1 copy-start.1
  163.3 0.7 copy-start.6
  163.3 149.4 %all-gather.13.cloned.1.call-start = ((), (), s32[]{:S(2)}) async-start(), calls=%async_computation.14 | async-start | bytes 3932160 | tf_op jit(solution)/shard_map/all_gather | solution.py:63
  244.6 38.8 %all-to-all-start.7 = ((bf16[64,8,704]{2,0,1:T(8,128)(2,1)}), bf16[64,8,704]{2,0,1:T(8,128)(2,1)}, u32[]{:S(2)}, u32[]{:S(2)}) async-start(bf16[64,8,704]{2,0,1:T(8,128)(2,1)} %copy.42), calls=%async_computation.7 | async-start | bytes 1572864 | tf_op jit(solution)/shard_map/all_to_all | solution.py:58
  248.8 93.9 %all-gather.15.cloned.1.call-start = ((), (), s32[]{:S(2)}) async-start(), calls=%async_computation.15 | async-start | bytes 3932160 | tf_op jit(solution)/shard_map/all_gather | solution.py:64
  285.0 0.8 copy-start.2
  288.5 98.2 %all-to-all-start.8 = ((bf16[8,128,2048]{2,1,0:T(8,128)(2,1)}), bf16[8,128,2048]{2,1,0:T(8,128)(2,1)}, u32[]{:S(2)}, u32[]{:S(2)}) async-start(bf16[8,128,2048]{2,1,0:T(8,128)(2,1)} %stack.2), calls=%async_computation.9 | async-start | bytes 8388608 | tf_op jit(solution)/shard_map/all_to_all | solution.py:9
  293.1 101.5 %all-gather.17.cloned.1.call-start = ((), (), s32[]{:S(2)}) async-start(), calls=%async_computation.16 | async-start | bytes 3604480 | tf_op jit(solution)/shard_map/all_gather | solution.py:74
  295.5 198.8 %reduce-scatter.5.cloned.1.call-start = ((), (), s32[]{:S(2)}) async-start(), calls=%async_computation.18 | async-start | bytes 4718592 | tf_op jit(solution)/shard_map/reduce_scatter | solution.py:90
  409.5 4.7 copy-start
  417.0 77.3 %copy-start.3 = (bf16[128,2048]{1,0:T(8,128)(2,1)S(1)}, bf16[128,2048]{1,0:T(8,128)(2,1)}, u32[]{:S(2)}) copy-start(bf16[128,2048]{1,0:T(8,128)(2,1)} %copy-done.2) | copy-start | bytes 1572868
  496.2 3.9 copy-start.4
Sparse Core Ops, SparseCore 0:
  51.4 31.6 all-gather.6
  94.9 26.6 all-gather.8
  123.7 27.0 all-gather.10
  163.4 119.4 reduce-scatter.2
  284.3 28.4 all-gather.12
  314.2 28.4 all-gather.14
  344.8 27.0 all-gather.16
  407.0 87.2 reduce-scatter.4
